TPU v7x, 32 devices: a whole 2x2x4 slice. The times are simulated.
32 devices in a mesh: fs: 4 (over z), tp: 4 (over y, x), rep: 2 (over core).
Axes of the slice: x: 2, y: 2, z: 4, core: 2. Of those that a mesh axis runs over, the one named last changes fastest.
Arguments:
- up_weight: float32 [2048, 8192], P('fs', ('tp', 'rep')), may hold values from -0.125 to 0.125
- up_momentum: float32 [2048, 8192], P('fs', ('tp', 'rep')), may hold values from -24 to 24
- up_grads: bfloat16 [2, 2048, 8192], P('rep', 'fs', 'tp'), may hold values from -2.09375 to 2.09375
- out_weight: float32 [2048, 2048], P('fs', ('tp', 'rep')), may hold values from -0.125 to 0.125
- out_momentum: float32 [2048, 2048], P('fs', ('tp', 'rep')), may hold values from -24 to 24
- out_grads: bfloat16 [2, 2048, 2048], P('rep', 'fs', 'tp'), may hold values from -2.09375 to 2.09375
Outputs:
- up_weight_new: float32 [2048, 8192], P('fs', ('tp', 'rep'))
- up_momentum_new: float32 [2048, 8192], P('fs', ('tp', 'rep'))
- up_direction: float32 [2048, 8192], P('fs', ('tp', 'rep'))
- out_weight_new: float32 [2048, 2048], P('fs', ('tp', 'rep'))
- out_momentum_new: float32 [2048, 2048], P('fs', ('tp', 'rep'))
- out_direction: float32 [2048, 2048], P('fs', ('tp', 'rep'))
All inputs are finite; a program needn't handle non-finite values.
Results may differ from a plain program's by a relative error of at most 0.039.
Values may be sent and summed in bfloat16 or wider, within the bound.
No kernel may reach another device: no remote copies, remote signals or barrier semaphores. Data moves between devices by JAX's collectives and lax.ppermute only.
A program may use at most 64 MiB of HBM per device.

v0:
```python
import math
import jax
import jax.numpy as jnp
from jax import lax
from jax.sharding import PartitionSpec as P

ITERS = 3
MOMENT = 0.9
RATE = 0.02
COEF_A = 3.4445
COEF_B = -4.775
COEF_C = 2.0315


def local_gram(values, columns):
    return lax.dot_general(
        values, columns, (((1,), (1,)), ((), ())), preferred_element_type=jnp.float32
    )


def contract(gram, values, gram_axis):
    return lax.dot_general(
        gram, values, (((gram_axis,), (0,)), ((), ())), preferred_element_type=jnp.float32
    )


def second_product(gram, first_half, gram_axis):
    return contract(gram, lax.all_gather(first_half, "fs", axis=0, tiled=True), gram_axis)


def on_device(up_weight, up_momentum, up_grads, out_weight, out_momentum, out_grads):
    grad_up, grad_out = (
        lax.psum_scatter(
            up_grads[0].astype(jnp.float32).astype(jnp.bfloat16),
            "rep",
            scatter_dimension=1,
            tiled=True,
        ).astype(jnp.float32),
        lax.psum_scatter(
            out_grads[0].astype(jnp.float32).astype(jnp.bfloat16),
            "rep",
            scatter_dimension=1,
            tiled=True,
        ).astype(jnp.float32),
    )
    moments = [MOMENT * up_momentum + grad_up, MOMENT * out_momentum + grad_out]
    group = lax.axis_size("tp") * lax.axis_size("rep")
    current = moments
    for iteration in range(ITERS):
        values = [entry.astype(jnp.bfloat16) for entry in current]
        columns = (
            lax.all_gather(values[0], "fs", axis=0, tiled=True),
            lax.all_gather(values[1], "fs", axis=0, tiled=True),
        )
        gram_sums = (
            lax.psum(local_gram(values[0], columns[0]).astype(jnp.bfloat16), ("tp", "rep")).astype(
                jnp.float32
            ),
            lax.psum(local_gram(values[1], columns[1]).astype(jnp.bfloat16), ("tp", "rep")).astype(
                jnp.float32
            ),
        )
        gram_axis = 1
        if iteration == 0:
            totals = lax.psum(
                (jnp.sum(gram_sums[0] * gram_sums[0]), jnp.sum(gram_sums[1] * gram_sums[1])), "fs"
            )
        if iteration == 0:
            squares = [1.0 / (jnp.sqrt(total) + 1.0) for total in totals]
            factors = [jnp.sqrt(square) for square in squares]
        else:
            squares = [1.0, 1.0]
            factors = [1.0, 1.0]
        halves = [(gram_sums[index] * squares[index]).astype(jnp.bfloat16) for index in range(2)]
        products = [
            factors[index] * contract(halves[index], columns[index], gram_axis)
            for index in range(2)
        ]
        seconds = [
            second_product(halves[index], products[index].astype(jnp.bfloat16), gram_axis)
            for index in range(2)
        ]
        current = [
            COEF_A * factors[index] * current[index]
            + COEF_B * products[index]
            + COEF_C * seconds[index]
            for index in range(2)
        ]
    widths = [up_weight.shape[1] * group, out_weight.shape[1] * group]
    directions = [current[index] * math.sqrt(widths[index]) for index in range(2)]
    return (
        up_weight - RATE * directions[0],
        moments[0],
        directions[0],
        out_weight - RATE * directions[1],
        moments[1],
        directions[1],
    )


def solution(mesh):
    return jax.shard_map(
        on_device,
        mesh=mesh,
        in_specs=(
            P("fs", ("tp", "rep")),
            P("fs", ("tp", "rep")),
            P("rep", "fs", "tp"),
            P("fs", ("tp", "rep")),
            P("fs", ("tp", "rep")),
            P("rep", "fs", "tp"),
        ),
        out_specs=(
            P("fs", ("tp", "rep")),
            P("fs", ("tp", "rep")),
            P("fs", ("tp", "rep")),
            P("fs", ("tp", "rep")),
            P("fs", ("tp", "rep")),
            P("fs", ("tp", "rep")),
        ),
        check_vma=False,
    )
```

profile of v0, /device:TPU:0, one launch (start us, length us, event | category | flops | bytes accessed | tf_op | source)
XLA Modules:
  0.0 994.7 jit_solution(5314064352922162735)
XLA Ops:
  8.7 12.2 %reduce-scatter.5.cloned.1.call-done = bf16[512,256]{1,0:T(8,128)(2,1)} async-done(((bf16[512,512]{1,0:T(8,128)(2,1)}), bf16[512,256]{1,0:T(8,128)(2,1)}) %reduce-scatter.5.cloned.1.call-update) | async-done | bytes 262160 | tf_op jit(solution)/shard_map/reduce_scatter | solution.py:39
  22.9 11.0 %reduce-scatter.3.cloned.1.call-done = bf16[512,1024]{1,0:T(8,128)(2,1)} async-done(((bf16[512,2048]{1,0:T(8,128)(2,1)}), bf16[512,1024]{1,0:T(8,128)(2,1)}) %reduce-scatter.3.cloned.1.call-update) | async-done | bytes 1048592 | tf_op jit(solution)/shard_map/reduce_scatter | solution.py:33
  33.9 3.3 fusion.26
  37.3 28.1 %all-gather.25.cloned.1.call-done = bf16[2048,256]{1,0:T(8,128)(2,1)} async-done(((bf16[512,256]{1,0:T(8,128)(2,1)}), bf16[2048,256]{1,0:T(8,128)(2,1)}) %all-gather.25.cloned.1.call-update) | async-done | bytes 1048592 | tf_op jit(solution)/shard_map/all_gather | solution.py:53
  68.7 78.9 %all-gather.13.cloned.1.call-done = bf16[2048,1024]{1,0:T(8,128)(2,1)} async-done(((bf16[512,1024]{1,0:T(8,128)(2,1)}), bf16[2048,1024]{1,0:T(8,128)(2,1)}) %all-gather.13.cloned.1.call-update) | async-done | bytes 4194320 | tf_op jit(solution)/shard_map/all_gather | solution.py:52
  147.5 5.9 convolution_convert_fusion.5
  153.5 79.4 %all-reduce.12.cloned.1.call-done = (bf16[512,2048]{1,0:T(8,128)(2,1)}, bf16[512,2048]{1,0:T(8,128)(2,1)}) async-done(((bf16[512,2048]{1,0:T(8,128)(2,1)}, bf16[512,2048]{1,0:T(8,128)(2,1)}), (bf16[512,2048]{1,0:T(8,128)(2,1)}, bf16[512,2048]{1,0:T(8,128)(2,1)})) %all-reduce.12.cloned.1.call-update) | async-done | bytes 4194320 | tf_op jit(solution)/shard_map/psum | solution.py:56
  232.9 4.0 fusion
  236.9 12.3 %all-reduce = (f32[]{:T(128)}, f32[]{:T(128)}) all-reduce(f32[]{:T(128)} %get-tuple-element.42, f32[]{:T(128)} %get-tuple-element.43), channel_id=1, replica_groups=mesh['fs'=4,'tp'=4,'rep'=2] {'fs'}, use_global_device_ids=true, to_apply=%region_3.0 | all-reduce | flops 2 | bytes 16 | tf_op jit(solution)/shard_map/psum | solution.py:65
  250.0 3.3 fusion.28
  254.2 6.3 multiply_convert_fusion
  260.6 18.3 %all-gather.27.cloned.1.call-done = bf16[2048,256]{1,0:T(8,128)(2,1)} async-done(((bf16[512,256]{1,0:T(8,128)(2,1)}), bf16[2048,256]{1,0:T(8,128)(2,1)}) %all-gather.27.cloned.1.call-update) | async-done | bytes 1048592 | tf_op jit(solution)/shard_map/all_gather | solution.py:28
  278.8 3.6 fusion.29
  282.5 78.6 %all-gather.15.cloned.1.call-done = bf16[2048,1024]{1,0:T(8,128)(2,1)} async-done(((bf16[512,1024]{1,0:T(8,128)(2,1)}), bf16[2048,1024]{1,0:T(8,128)(2,1)}) %all-gather.15.cloned.1.call-update) | async-done | bytes 4194320 | tf_op jit(solution)/shard_map/all_gather | solution.py:28
  361.1 7.6 fusion.27
  369.0 20.8 %all-gather.29.cloned.1.call-done = bf16[2048,256]{1,0:T(8,128)(2,1)} async-done(((bf16[512,256]{1,0:T(8,128)(2,1)}), bf16[2048,256]{1,0:T(8,128)(2,1)}) %all-gather.29.cloned.1.call-update) | async-done | bytes 1048592 | tf_op jit(solution)/shard_map/all_gather | solution.py:53
  393.1 79.0 %all-gather.17.cloned.1.call-done = bf16[2048,1024]{1,0:T(8,128)(2,1)} async-done(((bf16[512,1024]{1,0:T(8,128)(2,1)}), bf16[2048,1024]{1,0:T(8,128)(2,1)}) %all-gather.17.cloned.1.call-update) | async-done | bytes 4194320 | tf_op jit(solution)/shard_map/all_gather | solution.py:52
  472.1 5.9 convolution_convert_fusion.4
  478.0 79.4 %all-reduce.10.cloned.1.call-done = (bf16[512,2048]{1,0:T(8,128)(2,1)}, bf16[512,2048]{1,0:T(8,128)(2,1)}) async-done(((bf16[512,2048]{1,0:T(8,128)(2,1)}, bf16[512,2048]{1,0:T(8,128)(2,1)}), (bf16[512,2048]{1,0:T(8,128)(2,1)}, bf16[512,2048]{1,0:T(8,128)(2,1)})) %all-reduce.10.cloned.1.call-update) | async-done | bytes 4194320 | tf_op jit(solution)/shard_map/psum | solution.py:56
  560.6 6.9 fusion.30
  567.6 21.1 %all-gather.31.cloned.1.call-done = bf16[2048,256]{1,0:T(8,128)(2,1)} async-done(((bf16[512,256]{1,0:T(8,128)(2,1)}), bf16[2048,256]{1,0:T(8,128)(2,1)}) %all-gather.31.cloned.1.call-update) | async-done | bytes 1048592 | tf_op jit(solution)/shard_map/all_gather | solution.py:28
  591.6 78.7 %all-gather.19.cloned.1.call-done = bf16[2048,1024]{1,0:T(8,128)(2,1)} async-done(((bf16[512,1024]{1,0:T(8,128)(2,1)}), bf16[2048,1024]{1,0:T(8,128)(2,1)}) %all-gather.19.cloned.1.call-update) | async-done | bytes 4194320 | tf_op jit(solution)/shard_map/all_gather | solution.py:28
  670.3 8.4 fusion.31
  678.7 20.2 %all-gather.33.cloned.1.call-done = bf16[2048,256]{1,0:T(8,128)(2,1)} async-done(((bf16[512,256]{1,0:T(8,128)(2,1)}), bf16[2048,256]{1,0:T(8,128)(2,1)}) %all-gather.33.cloned.1.call-update) | async-done | bytes 1048592 | tf_op jit(solution)/shard_map/all_gather | solution.py:53
  698.9 3.3 convolution_convert_fusion
  702.2 78.3 %all-gather.21.cloned.1.call-done = bf16[2048,1024]{1,0:T(8,128)(2,1)} async-done(((bf16[512,1024]{1,0:T(8,128)(2,1)}), bf16[2048,1024]{1,0:T(8,128)(2,1)}) %all-gather.21.cloned.1.call-update) | async-done | bytes 4194320 | tf_op jit(solution)/shard_map/all_gather | solution.py:52
  780.5 5.9 convolution_convert_fusion.3
  786.4 79.4 %all-reduce.8.cloned.1.call-done = (bf16[512,2048]{1,0:T(8,128)(2,1)}, bf16[512,2048]{1,0:T(8,128)(2,1)}) async-done(((bf16[512,2048]{1,0:T(8,128)(2,1)}, bf16[512,2048]{1,0:T(8,128)(2,1)}), (bf16[512,2048]{1,0:T(8,128)(2,1)}, bf16[512,2048]{1,0:T(8,128)(2,1)})) %all-reduce.8.cloned.1.call-update) | async-done | bytes 4194320 | tf_op jit(solution)/shard_map/psum | solution.py:56
  869.2 7.0 fusion.34
  876.2 20.9 %all-gather.35.cloned.1.call-done = bf16[2048,256]{1,0:T(8,128)(2,1)} async-done(((bf16[512,256]{1,0:T(8,128)(2,1)}), bf16[2048,256]{1,0:T(8,128)(2,1)}) %all-gather.35.cloned.1.call-update) | async-done | bytes 1048592 | tf_op jit(solution)/shard_map/all_gather | solution.py:28
  900.2 78.5 %all-gather.23.cloned.1.call-done = bf16[2048,1024]{1,0:T(8,128)(2,1)} async-done(((bf16[512,1024]{1,0:T(8,128)(2,1)}), bf16[2048,1024]{1,0:T(8,128)(2,1)}) %all-gather.23.cloned.1.call-update) | async-done | bytes 4194320 | tf_op jit(solution)/shard_map/all_gather | solution.py:28
  978.7 9.5 broadcast_multiply_fusion
  (75 shorter events, 23.1 us)
Async XLA Ops:
  7.2 13.7 %reduce-scatter.5.cloned.1.call-start = ((), (), s32[]{:S(2)}) async-start(), calls=%async_computation.9 | async-start | bytes 786432 | tf_op jit(solution)/shard_map/reduce_scatter | solution.py:39
  7.9 26.0 %copy-start.7 = (f32[512,1024]{1,0:T(8,128)S(1)}, f32[512,1024]{1,0:T(8,128)}, u32[]{:S(2)}) copy-start(f32[512,1024]{1,0:T(8,128)} %param.7) | copy-start | bytes 6291460
  7.9 26.0 %reduce-scatter.3.cloned.1.call-start = ((), (), s32[]{:S(2)}) async-start(), calls=%async_computation.2 | async-start | bytes 3145728 | tf_op jit(solution)/shard_map/reduce_scatter | solution.py:33
  8.7 56.7 %all-gather.25.cloned.1.call-start = ((), (), s32[]{:S(2)}) async-start(), calls=%async_computation.10 | async-start | bytes 1310720 | tf_op jit(solution)/shard_map/all_gather | solution.py:53
  22.8 42.6 %copy-start.6 = (bf16[512,256]{1,0:T(8,128)(2,1)S(1)}, bf16[512,256]{1,0:T(8,128)(2,1)}, u32[]{:S(2)}) copy-start(bf16[512,256]{1,0:T(8,128)(2,1)} %get-tuple-element.14) | copy-start | bytes 786436
  22.8 124.7 %all-gather.13.cloned.1.call-start = ((), (), s32[]{:S(2)}) async-start(), calls=%async_computation.3 | async-start | bytes 5242880 | tf_op jit(solution)/shard_map/all_gather | solution.py:52
  37.2 110.3 %copy-start.4 = (bf16[512,1024]{1,0:T(8,128)(2,1)S(1)}, bf16[512,1024]{1,0:T(8,128)(2,1)}, u32[]{:S(2)}) copy-start(bf16[512,1024]{1,0:T(8,128)(2,1)} %get-tuple-element.16) | copy-start | bytes 3145732
  37.3 195.7 %all-reduce.12.cloned.1.call-start = ((), (), s32[]{:S(2)}) async-start(), calls=%async_computation.18 | async-start | bytes 8388608 | tf_op jit(solution)/shard_map/psum | solution.py:56
  153.4 125.4 %all-gather.27.cloned.1.call-start = ((), (), s32[]{:S(2)}) async-start(), calls=%async_computation.11 | async-start | bytes 1310720 | tf_op jit(solution)/shard_map/all_gather | solution.py:28
  232.9 17.1 %copy-start.10 = (bf16[2048,256]{1,0:T(8,128)(2,1)S(1)}, bf16[2048,256]{1,0:T(8,128)(2,1)}, u32[]{:S(2)}) copy-start(bf16[2048,256]{1,0:T(8,128)(2,1)} %all-gather.25.cloned.1.call-done) | copy-start | bytes 3145732
  253.4 107.8 %all-gather.15.cloned.1.call-start = ((), (), s32[]{:S(2)}) async-start(), calls=%async_computation.4 | async-start | bytes 5242880 | tf_op jit(solution)/shard_map/all_gather | solution.py:28
  254.2 24.7 %copy-start.15 = (f32[512,256]{1,0:T(8,128)S(1)}, f32[512,256]{1,0:T(8,128)}, u32[]{:S(2)}) copy-start(f32[512,256]{1,0:T(8,128)} %get-tuple-element.15) | copy-start | bytes 1572868
  254.2 24.6 %copy-start.16 = (f32[512,256]{1,0:T(8,128)S(1)}, f32[512,256]{1,0:T(8,128)}, u32[]{:S(2)}) copy-start(f32[512,256]{1,0:T(8,128)} %get-tuple-element.27) | copy-start | bytes 1572868
  260.5 129.3 %all-gather.29.cloned.1.call-start = ((), (), s32[]{:S(2)}) async-start(), calls=%async_computation.12 | async-start | bytes 1310720 | tf_op jit(solution)/shard_map/all_gather | solution.py:53
  278.8 82.3 %copy-start.8 = (f32[512,1024]{1,0:T(8,128)S(1)}, f32[512,1024]{1,0:T(8,128)}, u32[]{:S(2)}) copy-start(f32[512,1024]{1,0:T(8,128)} %get-tuple-element.17) | copy-start | bytes 6291460
  282.5 189.6 %all-gather.17.cloned.1.call-start = ((), (), s32[]{:S(2)}) async-start(), calls=%async_computation.5 | async-start | bytes 5242880 | tf_op jit(solution)/shard_map/all_gather | solution.py:52
  361.1 28.6 %copy-start.13 = (bf16[512,256]{1,0:T(8,128)(2,1)S(1)}, bf16[512,256]{1,0:T(8,128)(2,1)}, u32[]{:S(2)}) copy-start(bf16[512,256]{1,0:T(8,128)(2,1)} %get-tuple-element.28) | copy-start | bytes 786436
  368.7 103.4 %copy-start.11 = (bf16[512,1024]{1,0:T(8,128)(2,1)S(1)}, bf16[512,1024]{1,0:T(8,128)(2,1)}, u32[]{:S(2)}) copy-start(bf16[512,1024]{1,0:T(8,128)(2,1)} %get-tuple-element.24) | copy-start | bytes 3145732
  368.7 188.7 %all-reduce.10.cloned.1.call-start = ((), (), s32[]{:S(2)}) async-start(), calls=%async_computation.17 | async-start | bytes 8388608 | tf_op jit(solution)/shard_map/psum | solution.py:56
  477.9 79.5 %copy-start.2 = (bf16[2048,256]{1,0:T(8,128)(2,1)S(1)}, bf16[2048,256]{1,0:T(8,128)(2,1)}, u32[]{:S(2)}) copy-start(bf16[2048,256]{1,0:T(8,128)(2,1)} %all-gather.29.cloned.1.call-done) | copy-start | bytes 3145732
  478.0 110.7 %all-gather.31.cloned.1.call-start = ((), (), s32[]{:S(2)}) async-start(), calls=%async_computation.13 | async-start | bytes 1310720 | tf_op jit(solution)/shard_map/all_gather | solution.py:28
  560.5 109.8 %all-gather.19.cloned.1.call-start = ((), (), s32[]{:S(2)}) async-start(), calls=%async_computation.6 | async-start | bytes 5242880 | tf_op jit(solution)/shard_map/all_gather | solution.py:28
  560.5 28.2 %copy-start = (bf16[512,2048]{1,0:T(8,128)(2,1)S(1)}, bf16[512,2048]{1,0:T(8,128)(2,1)}, u32[]{:S(2)}) copy-start(bf16[512,2048]{1,0:T(8,128)(2,1)} %get-tuple-element.11) | copy-start | bytes 6291460
  567.5 131.4 %all-gather.33.cloned.1.call-start = ((), (), s32[]{:S(2)}) async-start(), calls=%async_computation.14 | async-start | bytes 1310720 | tf_op jit(solution)/shard_map/all_gather | solution.py:53
  591.5 189.0 %all-gather.21.cloned.1.call-start = ((), (), s32[]{:S(2)}) async-start(), calls=%async_computation.7 | async-start | bytes 5242880 | tf_op jit(solution)/shard_map/all_gather | solution.py:52
  670.3 28.6 %copy-start.5 = (bf16[512,256]{1,0:T(8,128)(2,1)S(1)}, bf16[512,256]{1,0:T(8,128)(2,1)}, u32[]{:S(2)}) copy-start(bf16[512,256]{1,0:T(8,128)(2,1)} %get-tuple-element.36) | copy-start | bytes 786436
  678.6 101.9 %copy-start.12 = (bf16[512,1024]{1,0:T(8,128)(2,1)S(1)}, bf16[512,1024]{1,0:T(8,128)(2,1)}, u32[]{:S(2)}) copy-start(bf16[512,1024]{1,0:T(8,128)(2,1)} %get-tuple-element.32) | copy-start | bytes 3145732
  678.6 187.2 %all-reduce.8.cloned.1.call-start = ((), (), s32[]{:S(2)}) async-start(), calls=%async_computation.16 | async-start | bytes 8388608 | tf_op jit(solution)/shard_map/psum | solution.py:56
  786.4 79.5 %copy-start.3 = (bf16[2048,256]{1,0:T(8,128)(2,1)S(1)}, bf16[2048,256]{1,0:T(8,128)(2,1)}, u32[]{:S(2)}) copy-start(bf16[2048,256]{1,0:T(8,128)(2,1)} %all-gather.33.cloned.1.call-done) | copy-start | bytes 3145732
  786.4 110.7 %all-gather.35.cloned.1.call-start = ((), (), s32[]{:S(2)}) async-start(), calls=%async_computation.15 | async-start | bytes 1310720 | tf_op jit(solution)/shard_map/all_gather | solution.py:28
  868.9 109.8 %all-gather.23.cloned.1.call-start = ((), (), s32[]{:S(2)}) async-start(), calls=%async_computation.8 | async-start | bytes 5242880 | tf_op jit(solution)/shard_map/all_gather | solution.py:28
  869.2 27.9 %copy-start.1 = (bf16[512,2048]{1,0:T(8,128)(2,1)S(1)}, bf16[512,2048]{1,0:T(8,128)(2,1)}, u32[]{:S(2)}) copy-start(bf16[512,2048]{1,0:T(8,128)(2,1)} %get-tuple-element.9) | copy-start | bytes 6291460
  (2 other events, 17.9 us)
Sparse Core Ops, SparseCore 0:
  10.2 10.6 reduce-scatter.4
  23.1 10.7 reduce-scatter.2
  36.1 29.2 all-gather.24
  67.4 80.1 all-gather.12
  153.5 79.3 all-reduce.11
  253.5 25.3 all-gather.26
  281.0 80.1 all-gather.14
  363.3 26.4 all-gather.28
  391.9 80.1 all-gather.16
  478.1 79.3 all-reduce.9
  560.6 28.0 all-gather.30
  590.1 80.1 all-gather.18
  672.4 26.4 all-gather.32
  700.3 80.0 all-gather.20
  786.5 79.3 all-reduce.7
  869.0 28.0 all-gather.34
  898.5 80.1 all-gather.22
where the time goes:
time: 995 us
  waiting for transfers between devices  864 us (87%)
  matrix products  91.9 us (9%)
  between operations  15.6 us (2%)
  blocking collectives  12.3 us (1%)
    all_gather x6, waiting for transfers between devices, second_product(): lax.all_gather(first_half, 'fs', axis=0, tiled=True)  296 us
    psum x3, waiting for transfers between devices, on_device(): lax.psum(local_gram(values[0], columns[0]).astype(jnp.bfloat16), ('tp', '...  238 us
    all_gather x3, waiting for transfers between devices, on_device(): lax.all_gather(values[0], 'fs', axis=0, tiled=True)  236 us
    all_gather x3, waiting for transfers between devices, on_device(): lax.all_gather(values[1], 'fs', axis=0, tiled=True)  69.1 us
    dot_general x12, matrix products, contract(): lax.dot_general(gram, values, (((gram_axis,), (0,)), ((), ())), preferred...  64.4 us
    dot_general x6, matrix products, local_gram(): lax.dot_general(values, columns, (((1,), (1,)), ((), ())), preferred_elem...  27.5 us
  transfers between devices with their start and end apart: 17, of which 17 were waited for; matrix products, arithmetic and copies ran while one was open for 6% of the time, Pallas kernels for 0%

commit v1 on v0

--- a/solution.py
+++ b/solution.py
@@ -53,9 +53,9 @@
             lax.all_gather(values[1], "fs", axis=0, tiled=True),
         )
         gram_sums = (
-            lax.psum(local_gram(values[0], columns[0]).astype(jnp.bfloat16), ("tp", "rep")).astype(
-                jnp.float32
-            ),
+            lax.psum(
+                lax.psum(local_gram(values[0], columns[0]).astype(jnp.bfloat16), "rep"), "tp"
+            ).astype(jnp.float32),
             lax.psum(local_gram(values[1], columns[1]).astype(jnp.bfloat16), ("tp", "rep")).astype(
                 jnp.float32
             ),

time: 995 us -> 1230 us (1.24)
  waiting for transfers between devices: 864 us -> 1090 us
    psum x3 -> x9, waiting for transfers between devices: 238 us -> 457 us  [the longest x3 206 us: on_device(): lax.psum(lax.psum(local_gram(values[0], columns[0]).astype(jnp.bfloat16),...]
  transfers between devices with their start and end apart: 17 -> 23, of which waited for: 17 -> 23; matrix products, arithmetic and copies ran while one was open for 6% -> 6% of each run, Pallas kernels for 0% -> 0%
where the time goes in v1:
time: 1230 us
  waiting for transfers between devices  1090 us (89%)
  matrix products  92.2 us (7%)
  between operations  15.7 us (1%)
  blocking collectives  12.3 us (1%)
    all_gather x6, waiting for transfers between devices, second_product(): lax.all_gather(first_half, 'fs', axis=0, tiled=True)  301 us
    all_gather x3, waiting for transfers between devices, on_device(): lax.all_gather(values[0], 'fs', axis=0, tiled=True)  236 us
    psum x3, waiting for transfers between devices, on_device(): lax.psum(lax.psum(local_gram(values[0], columns[0]).astype(jnp.bfloat16),...  206 us
    psum x3, waiting for transfers between devices, on_device(): lax.psum(local_gram(values[1], columns[1]).astype(jnp.bfloat16), ('tp', '...  190 us
    all_gather x3, waiting for transfers between devices, on_device(): lax.all_gather(values[1], 'fs', axis=0, tiled=True)  75.9 us
    dot_general x12, matrix products, contract(): lax.dot_general(gram, values, (((gram_axis,), (0,)), ((), ())), preferred...  64.1 us
    psum x3, waiting for transfers between devices, on_device(): lax.psum(local_gram(values[0], columns[0]).astype(jnp.bfloat16), 'rep')  61 us
    dot_general x6, matrix products, local_gram(): lax.dot_general(values, columns, (((1,), (1,)), ((), ())), preferred_elem...  28.1 us
  transfers between devices with their start and end apart: 23, of which 23 were waited for; matrix products, arithmetic and copies ran while one was open for 6% of the time, Pallas kernels for 0%

profile of v1, /device:TPU:0, one launch (start us, length us, event | category | flops | bytes accessed | tf_op | source)
XLA Modules:
  0.0 1226.3 jit_solution(3173638346339867813)
XLA Ops:
  8.7 13.9 %reduce-scatter.3.cloned.1.call-done = bf16[512,1024]{1,0:T(8,128)(2,1)} async-done(((bf16[512,2048]{1,0:T(8,128)(2,1)}), bf16[512,1024]{1,0:T(8,128)(2,1)}) %reduce-scatter.3.cloned.1.call-update) | async-done | bytes 1048592 | tf_op jit(solution)/shard_map/reduce_scatter | solution.py:33
  26.0 8.1 reduce-scatter.5.cloned.1.call-done
  36.1 82.1 %all-gather.13.cloned.1.call-done = bf16[2048,1024]{1,0:T(8,128)(2,1)} async-done(((bf16[512,1024]{1,0:T(8,128)(2,1)}), bf16[2048,1024]{1,0:T(8,128)(2,1)}) %all-gather.13.cloned.1.call-update) | async-done | bytes 4194320 | tf_op jit(solution)/shard_map/all_gather | solution.py:52
  124.1 22.5 %all-gather.25.cloned.1.call-done = bf16[2048,256]{1,0:T(8,128)(2,1)} async-done(((bf16[512,256]{1,0:T(8,128)(2,1)}), bf16[2048,256]{1,0:T(8,128)(2,1)}) %all-gather.25.cloned.1.call-update) | async-done | bytes 1048592 | tf_op jit(solution)/shard_map/all_gather | solution.py:53
  150.0 20.1 %all-reduce.11.cloned.1.call-done = bf16[512,2048]{1,0:T(8,128)(2,1)} async-done(((bf16[512,2048]{1,0:T(8,128)(2,1)}), bf16[512,2048]{1,0:T(8,128)(2,1)}) %all-reduce.11.cloned.1.call-update) | async-done | bytes 2097168 | tf_op jit(solution)/shard_map/psum | solution.py:57
  170.2 66.6 %all-reduce.23.cloned.1.call-done = bf16[512,2048]{1,0:T(8,128)(2,1)} async-done(((bf16[512,2048]{1,0:T(8,128)(2,1)}), bf16[512,2048]{1,0:T(8,128)(2,1)}) %all-reduce.23.cloned.1.call-update) | async-done | bytes 2097168 | tf_op jit(solution)/shard_map/psum | solution.py:59
  240.0 68.4 %all-reduce.13.cloned.1.call-done = bf16[512,2048]{1,0:T(8,128)(2,1)} async-done(((bf16[512,2048]{1,0:T(8,128)(2,1)}), bf16[512,2048]{1,0:T(8,128)(2,1)}) %all-reduce.13.cloned.1.call-update) | async-done | bytes 2097168 | tf_op jit(solution)/shard_map/psum | solution.py:56
  311.7 12.3 %all-reduce = (f32[]{:T(128)}, f32[]{:T(128)}) all-reduce(f32[]{:T(128)} %fusion, f32[]{:T(128)} %fusion.2), channel_id=1, replica_groups=mesh['fs'=4,'tp'=4,'rep'=2] {'fs'}, use_global_device_ids=true, to_apply=%region_4.0 | all-reduce | flops 2 | bytes 16 | tf_op jit(solution)/shard_map/psum | solution.py:65
  324.8 7.0 multiply_convert_fusion
  331.8 78.1 %all-gather.15.cloned.1.call-done = bf16[2048,1024]{1,0:T(8,128)(2,1)} async-done(((bf16[512,1024]{1,0:T(8,128)(2,1)}), bf16[2048,1024]{1,0:T(8,128)(2,1)}) %all-gather.15.cloned.1.call-update) | async-done | bytes 4194320 | tf_op jit(solution)/shard_map/all_gather | solution.py:28
  409.9 7.6 fusion.27
  421.9 75.0 %all-gather.17.cloned.1.call-done = bf16[2048,1024]{1,0:T(8,128)(2,1)} async-done(((bf16[512,1024]{1,0:T(8,128)(2,1)}), bf16[2048,1024]{1,0:T(8,128)(2,1)}) %all-gather.17.cloned.1.call-update) | async-done | bytes 4194320 | tf_op jit(solution)/shard_map/all_gather | solution.py:52
  497.0 6.0 convolution_convert_fusion.4
  503.0 22.4 %all-gather.27.cloned.1.call-done = bf16[2048,256]{1,0:T(8,128)(2,1)} async-done(((bf16[512,256]{1,0:T(8,128)(2,1)}), bf16[2048,256]{1,0:T(8,128)(2,1)}) %all-gather.27.cloned.1.call-update) | async-done | bytes 1048592 | tf_op jit(solution)/shard_map/all_gather | solution.py:28
  528.4 20.7 %all-reduce.15.cloned.1.call-done = bf16[512,2048]{1,0:T(8,128)(2,1)} async-done(((bf16[512,2048]{1,0:T(8,128)(2,1)}), bf16[512,2048]{1,0:T(8,128)(2,1)}) %all-reduce.15.cloned.1.call-update) | async-done | bytes 2097168 | tf_op jit(solution)/shard_map/psum | solution.py:57
  549.2 31.1 %all-gather.29.cloned.1.call-done = bf16[2048,256]{1,0:T(8,128)(2,1)} async-done(((bf16[512,256]{1,0:T(8,128)(2,1)}), bf16[2048,256]{1,0:T(8,128)(2,1)}) %all-gather.29.cloned.1.call-update) | async-done | bytes 1048592 | tf_op jit(solution)/shard_map/all_gather | solution.py:53
  583.8 68.5 %all-reduce.17.cloned.1.call-done = bf16[512,2048]{1,0:T(8,128)(2,1)} async-done(((bf16[512,2048]{1,0:T(8,128)(2,1)}), bf16[512,2048]{1,0:T(8,128)(2,1)}) %all-reduce.17.cloned.1.call-update) | async-done | bytes 2097168 | tf_op jit(solution)/shard_map/psum | solution.py:56
  652.3 6.8 fusion.28
  659.2 58.0 %all-reduce.25.cloned.1.call-done = bf16[512,2048]{1,0:T(8,128)(2,1)} async-done(((bf16[512,2048]{1,0:T(8,128)(2,1)}), bf16[512,2048]{1,0:T(8,128)(2,1)}) %all-reduce.25.cloned.1.call-update) | async-done | bytes 2097168 | tf_op jit(solution)/shard_map/psum | solution.py:59
  720.3 78.2 %all-gather.19.cloned.1.call-done = bf16[2048,1024]{1,0:T(8,128)(2,1)} async-done(((bf16[512,1024]{1,0:T(8,128)(2,1)}), bf16[2048,1024]{1,0:T(8,128)(2,1)}) %all-gather.19.cloned.1.call-update) | async-done | bytes 4194320 | tf_op jit(solution)/shard_map/all_gather | solution.py:28
  798.5 8.4 fusion.29
  807.0 20.0 %all-gather.31.cloned.1.call-done = bf16[2048,256]{1,0:T(8,128)(2,1)} async-done(((bf16[512,256]{1,0:T(8,128)(2,1)}), bf16[2048,256]{1,0:T(8,128)(2,1)}) %all-gather.31.cloned.1.call-update) | async-done | bytes 1048592 | tf_op jit(solution)/shard_map/all_gather | solution.py:28
  829.8 78.7 %all-gather.21.cloned.1.call-done = bf16[2048,1024]{1,0:T(8,128)(2,1)} async-done(((bf16[512,1024]{1,0:T(8,128)(2,1)}), bf16[2048,1024]{1,0:T(8,128)(2,1)}) %all-gather.21.cloned.1.call-update) | async-done | bytes 4194320 | tf_op jit(solution)/shard_map/all_gather | solution.py:52
  908.5 6.2 convolution_convert_fusion.3
  914.8 22.2 %all-gather.33.cloned.1.call-done = bf16[2048,256]{1,0:T(8,128)(2,1)} async-done(((bf16[512,256]{1,0:T(8,128)(2,1)}), bf16[2048,256]{1,0:T(8,128)(2,1)}) %all-gather.33.cloned.1.call-update) | async-done | bytes 1048592 | tf_op jit(solution)/shard_map/all_gather | solution.py:53
  940.5 20.2 %all-reduce.19.cloned.1.call-done = bf16[512,2048]{1,0:T(8,128)(2,1)} async-done(((bf16[512,2048]{1,0:T(8,128)(2,1)}), bf16[512,2048]{1,0:T(8,128)(2,1)}) %all-reduce.19.cloned.1.call-update) | async-done | bytes 2097168 | tf_op jit(solution)/shard_map/psum | solution.py:57
  960.9 65.8 %all-reduce.27.cloned.1.call-done = bf16[512,2048]{1,0:T(8,128)(2,1)} async-done(((bf16[512,2048]{1,0:T(8,128)(2,1)}), bf16[512,2048]{1,0:T(8,128)(2,1)}) %all-reduce.27.cloned.1.call-update) | async-done | bytes 2097168 | tf_op jit(solution)/shard_map/psum | solution.py:59
  1029.8 68.6 %all-reduce.21.cloned.1.call-done = bf16[512,2048]{1,0:T(8,128)(2,1)} async-done(((bf16[512,2048]{1,0:T(8,128)(2,1)}), bf16[512,2048]{1,0:T(8,128)(2,1)}) %all-reduce.21.cloned.1.call-update) | async-done | bytes 2097168 | tf_op jit(solution)/shard_map/psum | solution.py:56
  1098.4 6.8 fusion.30
  1105.2 23.3 %all-gather.35.cloned.1.call-done = bf16[2048,256]{1,0:T(8,128)(2,1)} async-done(((bf16[512,256]{1,0:T(8,128)(2,1)}), bf16[2048,256]{1,0:T(8,128)(2,1)}) %all-gather.35.cloned.1.call-update) | async-done | bytes 1048592 | tf_op jit(solution)/shard_map/all_gather | solution.py:28
  1131.6 78.6 %all-gather.23.cloned.1.call-done = bf16[2048,1024]{1,0:T(8,128)(2,1)} async-done(((bf16[512,1024]{1,0:T(8,128)(2,1)}), bf16[2048,1024]{1,0:T(8,128)(2,1)}) %all-gather.23.cloned.1.call-update) | async-done | bytes 4194320 | tf_op jit(solution)/shard_map/all_gather | solution.py:28
  1210.3 9.5 broadcast_multiply_fusion
  (92 shorter events, 48.8 us)
Async XLA Ops:
  7.2 15.4 %reduce-scatter.3.cloned.1.call-start = ((), (), s32[]{:S(2)}) async-start(), calls=%async_computation.2 | async-start | bytes 3145728 | tf_op jit(solution)/shard_map/reduce_scatter | solution.py:33
  7.9 26.2 %reduce-scatter.5.cloned.1.call-start = ((), (), s32[]{:S(2)}) async-start(), calls=%async_computation.15 | async-start | bytes 786432 | tf_op jit(solution)/shard_map/reduce_scatter | solution.py:39
  8.7 109.5 %all-gather.13.cloned.1.call-start = ((), (), s32[]{:S(2)}) async-start(), calls=%async_computation.3 | async-start | bytes 5242880 | tf_op jit(solution)/shard_map/all_gather | solution.py:52
  25.9 92.2 %copy-start.4 = (bf16[512,1024]{1,0:T(8,128)(2,1)S(1)}, bf16[512,1024]{1,0:T(8,128)(2,1)}, u32[]{:S(2)}) copy-start(bf16[512,1024]{1,0:T(8,128)(2,1)} %get-tuple-element.10) | copy-start | bytes 3145732
  25.9 120.7 %all-gather.25.cloned.1.call-start = ((), (), s32[]{:S(2)}) async-start(), calls=%async_computation.16 | async-start | bytes 1310720 | tf_op jit(solution)/shard_map/all_gather | solution.py:53
  36.0 134.1 %all-reduce.11.cloned.1.call-start = ((), (), s32[]{:S(2)}) async-start(), calls=%async_computation.4 | async-start | bytes 4194304 | tf_op jit(solution)/shard_map/psum | solution.py:57
  124.0 112.7 %all-reduce.23.cloned.1.call-start = ((), (), s32[]{:S(2)}) async-start(), calls=%async_computation.17 | async-start | bytes 4194304 | tf_op jit(solution)/shard_map/psum | solution.py:59
  149.9 158.5 %all-reduce.13.cloned.1.call-start = ((), (), s32[]{:S(2)}) async-start(), calls=%async_computation.5 | async-start | bytes 4194304 | tf_op jit(solution)/shard_map/psum | solution.py:56
  170.1 239.8 %all-gather.15.cloned.1.call-start = ((), (), s32[]{:S(2)}) async-start(), calls=%async_computation.6 | async-start | bytes 5242880 | tf_op jit(solution)/shard_map/all_gather | solution.py:28
  324.8 85.1 %copy-start.8 = (f32[512,1024]{1,0:T(8,128)S(1)}, f32[512,1024]{1,0:T(8,128)}, u32[]{:S(2)}) copy-start(f32[512,1024]{1,0:T(8,128)} %get-tuple-element.11) | copy-start | bytes 6291460
  331.8 165.2 %all-gather.17.cloned.1.call-start = ((), (), s32[]{:S(2)}) async-start(), calls=%async_computation.7 | async-start | bytes 5242880 | tf_op jit(solution)/shard_map/all_gather | solution.py:52
  417.6 107.9 %all-gather.27.cloned.1.call-start = ((), (), s32[]{:S(2)}) async-start(), calls=%async_computation.18 | async-start | bytes 1310720 | tf_op jit(solution)/shard_map/all_gather | solution.py:28
  418.4 78.6 %copy-start.11 = (bf16[512,1024]{1,0:T(8,128)(2,1)S(1)}, bf16[512,1024]{1,0:T(8,128)(2,1)}, u32[]{:S(2)}) copy-start(bf16[512,1024]{1,0:T(8,128)(2,1)} %get-tuple-element.18) | copy-start | bytes 3145732
  421.7 127.4 %all-reduce.15.cloned.1.call-start = ((), (), s32[]{:S(2)}) async-start(), calls=%async_computation.8 | async-start | bytes 4194304 | tf_op jit(solution)/shard_map/psum | solution.py:57
  497.0 28.5 %copy-start.15 = (f32[512,256]{1,0:T(8,128)S(1)}, f32[512,256]{1,0:T(8,128)}, u32[]{:S(2)}) copy-start(f32[512,256]{1,0:T(8,128)} %get-tuple-element.27) | copy-start | bytes 1572868
  502.9 77.3 %all-gather.29.cloned.1.call-start = ((), (), s32[]{:S(2)}) async-start(), calls=%async_computation.19 | async-start | bytes 1310720 | tf_op jit(solution)/shard_map/all_gather | solution.py:53
  528.3 52.0 %copy-start.12 = (bf16[512,256]{1,0:T(8,128)(2,1)S(1)}, bf16[512,256]{1,0:T(8,128)(2,1)}, u32[]{:S(2)}) copy-start(bf16[512,256]{1,0:T(8,128)(2,1)} %get-tuple-element.28) | copy-start | bytes 786436
  528.3 124.0 %all-reduce.17.cloned.1.call-start = ((), (), s32[]{:S(2)}) async-start(), calls=%async_computation.9 | async-start | bytes 4194304 | tf_op jit(solution)/shard_map/psum | solution.py:56
  549.1 168.1 %all-reduce.25.cloned.1.call-start = ((), (), s32[]{:S(2)}) async-start(), calls=%async_computation.20 | async-start | bytes 4194304 | tf_op jit(solution)/shard_map/psum | solution.py:59
  583.7 133.5 %copy-start.2 = (bf16[2048,256]{1,0:T(8,128)(2,1)S(1)}, bf16[2048,256]{1,0:T(8,128)(2,1)}, u32[]{:S(2)}) copy-start(bf16[2048,256]{1,0:T(8,128)(2,1)} %all-gather.29.cloned.1.call-done) | copy-start | bytes 3145732
  583.7 214.7 %all-gather.19.cloned.1.call-start = ((), (), s32[]{:S(2)}) async-start(), calls=%async_computation.10 | async-start | bytes 5242880 | tf_op jit(solution)/shard_map/all_gather | solution.py:28
  659.1 167.8 %all-gather.31.cloned.1.call-start = ((), (), s32[]{:S(2)}) async-start(), calls=%async_computation.21 | async-start | bytes 1310720 | tf_op jit(solution)/shard_map/all_gather | solution.py:28
  720.2 188.3 %all-gather.21.cloned.1.call-start = ((), (), s32[]{:S(2)}) async-start(), calls=%async_computation.11 | async-start | bytes 5242880 | tf_op jit(solution)/shard_map/all_gather | solution.py:52
  798.4 28.5 %copy-start = (bf16[512,2048]{1,0:T(8,128)(2,1)S(1)}, bf16[512,2048]{1,0:T(8,128)(2,1)}, u32[]{:S(2)}) copy-start(bf16[512,2048]{1,0:T(8,128)(2,1)} %all-reduce.25.cloned.1.call-done) | copy-start | bytes 6291460
  806.9 130.1 %all-gather.33.cloned.1.call-start = ((), (), s32[]{:S(2)}) async-start(), calls=%async_computation.22 | async-start | bytes 1310720 | tf_op jit(solution)/shard_map/all_gather | solution.py:53
  829.8 130.9 %all-reduce.19.cloned.1.call-start = ((), (), s32[]{:S(2)}) async-start(), calls=%async_computation.12 | async-start | bytes 4194304 | tf_op jit(solution)/shard_map/psum | solution.py:57
  914.7 112.0 %all-reduce.27.cloned.1.call-start = ((), (), s32[]{:S(2)}) async-start(), calls=%async_computation.23 | async-start | bytes 4194304 | tf_op jit(solution)/shard_map/psum | solution.py:59
  940.4 86.3 %copy-start.3 = (bf16[2048,256]{1,0:T(8,128)(2,1)S(1)}, bf16[2048,256]{1,0:T(8,128)(2,1)}, u32[]{:S(2)}) copy-start(bf16[2048,256]{1,0:T(8,128)(2,1)} %all-gather.33.cloned.1.call-done) | copy-start | bytes 3145732
  940.4 158.0 %all-reduce.21.cloned.1.call-start = ((), (), s32[]{:S(2)}) async-start(), calls=%async_computation.13 | async-start | bytes 4194304 | tf_op jit(solution)/shard_map/psum | solution.py:56
  960.7 167.9 %all-gather.35.cloned.1.call-start = ((), (), s32[]{:S(2)}) async-start(), calls=%async_computation.24 | async-start | bytes 1310720 | tf_op jit(solution)/shard_map/all_gather | solution.py:28
  1029.7 98.8 %copy-start.1 = (bf16[512,2048]{1,0:T(8,128)(2,1)S(1)}, bf16[512,2048]{1,0:T(8,128)(2,1)}, u32[]{:S(2)}) copy-start(bf16[512,2048]{1,0:T(8,128)(2,1)} %all-reduce.27.cloned.1.call-done) | copy-start | bytes 6291460
  1029.7 180.5 %all-gather.23.cloned.1.call-start = ((), (), s32[]{:S(2)}) async-start(), calls=%async_computation.14 | async-start | bytes 5242880 | tf_op jit(solution)/shard_map/all_gather | solution.py:28
  (7 other events, 145.3 us)
Sparse Core Ops, SparseCore 0:
  10.2 12.3 reduce-scatter.2
  24.8 9.2 reduce-scatter.4
  36.2 81.8 all-gather.12
  120.1 26.4 all-gather.24
  149.4 20.6 all-reduce.10
  173.8 62.9 all-reduce.22
  239.8 68.5 all-reduce.12
  331.9 77.9 all-gather.14
  417.7 79.2 all-gather.16
  498.9 26.4 all-gather.26
  528.4 20.6 all-reduce.14
  551.1 29.1 all-gather.28
  583.4 68.8 all-reduce.16
  655.4 61.7 all-reduce.24
  718.6 79.8 all-gather.18
  800.4 26.4 all-gather.30
  828.4 80.1 all-gather.20
  910.5 26.4 all-gather.32
  939.9 20.6 all-reduce.18
  963.7 62.9 all-reduce.26
  1029.8 68.5 all-reduce.20
  1100.5 27.9 all-gather.34
  1130.1 80.1 all-gather.22
